TPU v7x, 32 devices: a whole 2x2x4 slice. The times are simulated.
32 devices in a mesh: ep: 4 (over y, x), tp: 8 (over z, core).
Axes of the slice: x: 2, y: 2, z: 4, core: 2. Of those that a mesh axis runs over, the one named last changes fastest.
Arguments:
- queries: bfloat16 [2048, 16, 128], P('ep', 'tp'), may hold values from -125 to 125
- keys: bfloat16 [2048, 16, 128], P('ep', 'tp'), may hold values from -9 to 9
- values: bfloat16 [2048, 16, 128], P('ep', 'tp'), may hold values from -6 to 6
- mixing: float32 [16], P('tp'), may hold values from 0.3 to 0.8
- head_gain: float32 [128], replicated, may hold values from 0.1 to 1.9
- out_weight: bfloat16 [16, 128, 2048], P('tp'), may hold values from -0.125 to 0.125
- tokens_b: bfloat16 [4096, 2048], P(('ep', 'tp')), may hold values from -6 to 6
- norm_gain: float32 [2048], replicated, may hold values from 0.1 to 1.9
- expert_ids: int32 [4096, 2], P(('ep', 'tp')), may hold values from 0 to 3, all different within a row; in each aligned block of 128 rows (0 to 127, 128 to 255, ...) at most 96 rows name the same one
- group_gate: float32 [4096], P(('ep', 'tp')), may hold values from 0.2 to 1
- expert_gate: float32 [4096, 2], P(('ep', 'tp')), may hold values from 0.1 to 0.9
- gate_weight: bfloat16 [4, 2048, 1024], P('ep', None, 'tp'), may hold values from -0.125 to 0.125
- up_weight: bfloat16 [4, 2048, 1024], P('ep', None, 'tp'), may hold values from -0.125 to 0.125
- down_weight: bfloat16 [4, 2048, 1024], P('ep', None, 'tp'), may hold values from -0.1875 to 0.1875
Outputs:
- mixed: bfloat16 [2048, 2048], P(('ep', 'tp'))
- routed: bfloat16 [4096, 2048], P(('ep', 'tp'))
Inputs may be any that keep to these rules, and one draw needn't show every extreme that they name: `expert_ids`: within each aligned block of 128 rows, no expert is named by more than 96 rows, and some block has an expert named by exactly 96 rows.
All inputs are finite; a program needn't handle non-finite values.
Results may differ from a plain program's by a relative error of at most 0.019.
Values may be sent and summed in bfloat16 or wider, within the bound.
A program may use at most 192 MiB of HBM per device.

v0:
```python
import math
import jax
import jax.numpy as jnp
from jax import lax
from jax.sharding import PartitionSpec as P

HEAD = 64


def attend_heads(queries, keys, values, mixing, head_gain):
    shard_rows = queries.shape[0]
    head_count = queries.shape[1]
    value_width = values.shape[2]
    query_start = lax.axis_index("ep") * shard_rows
    score_scale = 1.0 / math.sqrt(HEAD)
    query_pos = query_start + lax.iota(jnp.int32, shard_rows)

    def update(running, key_block, value_block, block_start):
        key_pos = block_start + lax.iota(jnp.int32, shard_rows)
        allowed = key_pos[None, :] <= query_pos[:, None]
        fresh = []
        for map_index in range(2):
            maximum, row_sum, numerator = running[3 * map_index : 3 * map_index + 3]
            offset = map_index * HEAD
            scores = (
                jnp.einsum(
                    "qhd,khd->hqk",
                    queries[:, :, offset : offset + HEAD],
                    key_block[:, :, offset : offset + HEAD],
                    preferred_element_type=jnp.float32,
                )
                * score_scale
            )
            scores = jnp.where(allowed[None], scores, -1e30)
            newmax = jnp.maximum(maximum, jnp.max(scores, axis=2))
            shrink = jnp.exp(maximum - newmax)
            weights = jnp.exp(scores - newmax[:, :, None])
            row_sum = row_sum * shrink + jnp.sum(weights, axis=2)
            numerator = numerator * shrink[:, :, None] + jnp.einsum(
                "hqk,khe->hqe",
                weights.astype(jnp.bfloat16),
                value_block,
                preferred_element_type=jnp.float32,
            )
            fresh += [newmax, row_sum, numerator]
        return tuple(fresh)

    floor_max = jnp.full((head_count, shard_rows), -1e30, jnp.float32)
    zero_sum = jnp.zeros((head_count, shard_rows), jnp.float32)
    zero_acc = jnp.zeros((head_count, shard_rows, value_width), jnp.float32)
    start_state = (floor_max, zero_sum, zero_acc, floor_max, zero_sum, zero_acc)
    running = start_state
    key_piece = lax.all_gather(keys, "ep", axis=0, tiled=True)
    value_piece = lax.all_gather(values, "ep", axis=0, tiled=True)
    blocks = key_piece.shape[0] // shard_rows
    key_blocks = key_piece.reshape(blocks, shard_rows, head_count, key_piece.shape[2])
    value_blocks = value_piece.reshape(blocks, shard_rows, head_count, value_width)

    def visit_block(state, inputs):
        key_block, value_block, block_index = inputs
        block_start = block_index * shard_rows
        state = lax.cond(
            block_start <= query_start + shard_rows - 1,
            lambda state_in: update(state_in, key_block, value_block, block_start),
            lambda state_in: state_in,
            state,
        )
        return (state, None)

    running, unused = lax.scan(
        visit_block, running, (key_blocks, value_blocks, lax.iota(jnp.int32, blocks))
    )
    state = running
    diff = state[2] / state[1][:, :, None] - mixing[:, None, None] * state[5] / state[4][:, :, None]
    normed = diff * lax.rsqrt(jnp.mean(diff * diff, axis=2, keepdims=True) + 1e-05) * head_gain
    return normed.astype(jnp.bfloat16)


def mixer_half(queries, keys, values, mixing, head_gain, out_weight):
    attended = attend_heads(queries, keys, values, mixing, head_gain)
    return lax.psum_scatter(
        jnp.einsum("hqe,hed->qd", attended, out_weight, preferred_element_type=jnp.float32).astype(
            jnp.bfloat16
        ),
        "tp",
        scatter_dimension=0,
        tiled=True,
    )


def expert_half(
    tokens_b, norm_gain, expert_ids, group_gate, expert_gate, gate_weight, up_weight, down_weight
):
    local_rows = tokens_b.shape[0]
    width = tokens_b.shape[1]
    top_count = expert_ids.shape[1]
    ep_count = lax.axis_size("ep")
    local_count = gate_weight.shape[0]
    expert_total = ep_count * local_count
    capacity = 3 * local_rows * top_count // (2 * expert_total)
    tokens_f = tokens_b.astype(jnp.float32)
    normed = (
        tokens_f
        * lax.rsqrt(jnp.mean(tokens_f * tokens_f, axis=1, keepdims=True) + 1e-06)
        * norm_gain
    ).astype(jnp.bfloat16)
    flat_ids = expert_ids.reshape(-1)
    one_hot = (flat_ids[:, None] == lax.iota(jnp.int32, expert_total)[None, :]).astype(jnp.int32)
    slot_rank = jnp.sum((jnp.cumsum(one_hot, axis=0) - one_hot) * one_hot, axis=1)
    slot_index = flat_ids * capacity + slot_rank
    owners = jnp.full((expert_total * capacity,), local_rows, jnp.int32)
    owners = owners.at[slot_index].set(lax.iota(jnp.int32, local_rows * top_count) // top_count)
    padded = jnp.concatenate([normed, jnp.zeros((1, width), jnp.bfloat16)], axis=0)
    outgoing = padded[owners].reshape(ep_count, local_count * capacity, width)
    incoming = lax.all_to_all(outgoing, "ep", split_axis=0, concat_axis=0, tiled=True)
    expert_rows = jnp.transpose(
        incoming.reshape(ep_count, local_count, capacity, width), (1, 0, 2, 3)
    )
    expert_rows = expert_rows.reshape(local_count, ep_count * capacity, width)
    piece_gate = lax.all_gather(gate_weight, "tp", axis=2, tiled=True)
    piece_up = lax.all_gather(up_weight, "tp", axis=2, tiled=True)
    piece_down = lax.all_gather(down_weight, "tp", axis=2, tiled=True)
    gate_part = jnp.einsum(
        "jrd,jdf->jrf", expert_rows, piece_gate, preferred_element_type=jnp.float32
    )
    up_part = jnp.einsum("jrd,jdf->jrf", expert_rows, piece_up, preferred_element_type=jnp.float32)
    hidden = (jax.nn.silu(gate_part) * up_part).astype(jnp.bfloat16)
    expert_out = jnp.einsum(
        "jrf,jdf->jrd", hidden, piece_down, preferred_element_type=jnp.float32
    ).astype(jnp.bfloat16)
    outbound = jnp.transpose(
        expert_out.reshape(local_count, ep_count, capacity, width), (1, 0, 2, 3)
    )
    outbound = outbound.reshape(ep_count, local_count * capacity, width)
    returned = lax.all_to_all(outbound, "ep", split_axis=0, concat_axis=0, tiled=True).reshape(
        expert_total * capacity, width
    )
    picked = returned[slot_index].reshape(local_rows, top_count, width).astype(jnp.float32)
    route_weight = group_gate[:, None] * expert_gate
    return jnp.sum(route_weight[:, :, None] * picked, axis=1).astype(jnp.bfloat16)


def per_device(
    queries,
    keys,
    values,
    mixing,
    head_gain,
    out_weight,
    tokens_b,
    norm_gain,
    expert_ids,
    group_gate,
    expert_gate,
    gate_weight,
    up_weight,
    down_weight,
):
    mixed = mixer_half(queries, keys, values, mixing, head_gain, out_weight)
    routed = expert_half(
        tokens_b,
        norm_gain,
        expert_ids,
        group_gate,
        expert_gate,
        gate_weight,
        up_weight,
        down_weight,
    )
    return (mixed, routed)


def solution(mesh):
    placed = (
        P("ep", "tp", None),
        P("ep", "tp", None),
        P("ep", "tp", None),
        P("tp"),
        P(),
        P("tp", None, None),
        P(("ep", "tp"), None),
        P(),
        P(("ep", "tp"), None),
        P(("ep", "tp")),
        P(("ep", "tp"), None),
        P("ep", None, "tp"),
        P("ep", None, "tp"),
        P("ep", None, "tp"),
    )
    return jax.shard_map(
        per_device,
        mesh=mesh,
        in_specs=placed,
        out_specs=(P(("ep", "tp"), None), P(("ep", "tp"), None)),
        check_vma=False,
    )
```

profile of v0, /device:TPU:0, one launch (start us, length us, event | category | flops | bytes accessed | tf_op | source)
XLA Modules:
  0.0 260.2 jit_solution(6079203360803837472)
XLA Ops:
  7.2 0.0 copy-start
  7.2 0.0 all-gather.6.cloned.1.call-start
  7.3 1.8 copy.24
  9.1 0.0 all-gather.6.cloned.1.call-update
  9.1 0.0 all-gather.8.cloned.1.call-start
  9.1 1.7 copy.25
  10.8 0.0 all-gather.8.cloned.1.call-update
  10.8 0.0 all-gather.10.cloned.1.call-start
  10.9 0.7 all-gather.10.cloned.1.call-update
  11.6 0.0 all-gather.12.cloned.1.call-start
  11.6 0.5 all-gather.12.cloned.1.call-update
  12.2 0.0 all-gather.14.cloned.1.call-start
  12.2 0.5 all-gather.14.cloned.1.call-update
  12.7 0.0 reduce-scatter.2.cloned.1.call-start
  12.8 0.1 copy.31
  12.9 0.1 eq.29
  13.1 0.1 eq.25
  13.2 0.2 copy.27
  13.4 1.2 reduce-window.6
  14.6 0.1 slice.34
  14.7 0.1 copy.33
  14.9 0.1 copy.34
  15.0 0.1 copy.30
  15.1 0.1 mul.169
  15.2 0.1 add_bitcast_fusion
  15.3 1.4 scatter_custom_fusion
  16.7 0.2 fusion.31
  17.0 1.0 fusion.33
  17.9 21.8 %all-gather.6.cloned.1.call-done = bf16[2048,2,128]{2,0,1:T(8,128)(2,1)} async-done(((bf16[512,2,128]{2,0,1:T(8,128)(2,1)}), bf16[2048,2,128]{2,0,1:T(8,128)(2,1)}) %all-gather.6.cloned.1.call-update) | async-done | bytes 1048592 | tf_op jit(solution)/shard_map/all_gather | solution.py:53
  39.7 2.3 copy.26
  42.0 26.1 %all-gather.8.cloned.1.call-done = bf16[2048,2,128]{2,0,1:T(8,128)(2,1)} async-done(((bf16[512,2,128]{2,0,1:T(8,128)(2,1)}), bf16[2048,2,128]{2,0,1:T(8,128)(2,1)}) %all-gather.8.cloned.1.call-update) | async-done | bytes 1048592 | tf_op jit(solution)/shard_map/all_gather | solution.py:54
  68.1 1.3 copy.28
  69.5 0.0 copy-start.8
  69.5 0.0 copy-start.9
  69.5 9.8 %while.23 = (s32[]{:T(128)}, f32[2,512]{1,0:T(2,128)S(1)}, f32[2,512]{1,0:T(2,128)S(1)}, f32[2,512,128]{2,1,0:T(8,128)S(1)}, f32[2,512]{1,0:T(2,128)S(1)}, /*ind...) while((s32[]{:T(128)}, f32[2,512]{1,0:T(2,128)S(1)}, ...), condition=%wide.region_7.8_spmd.clone, body=%wide.region_0.7_spmd.clone.sunk | while | flops 410784768 | bytes 17183128 | solution.py:70
  69.6 0.6 dynamic_slice.36
  70.8 4.6 %conditional.3 = ((f32[2,512]{1,0:T(2,128)S(1)}, f32[2,512]{1,0:T(2,128)S(1)}, f32[2,512,128]{2,1,0:T(8,128)S(1)}, f32[2,512]{1,0:T(2,128)S(1)}, f32[2,512]{1,0:T(2,128)S(1)}, /*index=5*/f32[2,512,128]{2,1,0:T(8,128)S(1)})) conditional(s32[]{:T(128)} %convert_element_type.87, (f32[2,512]{1,0:T(2,128)S(1)}, f32[2,512]{1,0:T(2,128)S(1)}, ...), branch_computations={%region_1.1_spmd, %region_2.6_spmd} | conditional | flops 410784768 | bytes 17180748 | solution.py:62
  70.8 1.0 dynamic-slice_bitcast_fusion
  71.8 0.2 broadcast_compare_fusion
  72.1 0.6 fusion.45
  72.7 0.3 fusion.3
  73.0 0.6 fusion.46
  73.6 0.3 fusion.5
  74.0 0.7 convolution_add_fusion
  74.7 0.7 convolution_add_fusion.1
  75.5 0.6 dynamic_slice.36
  76.8 0.6 dynamic_slice.36
  78.1 0.6 dynamic_slice.36
  79.4 0.5 multiply_reduce_fusion.1
  79.9 0.0 copy-start.2
  79.9 2.1 bitcast_convert_fusion
  82.0 0.0 reduce-scatter.2.cloned.1.call-update
  82.2 2.5 gather_fusion
  84.6 36.1 %all_to_all.10 = bf16[4,96,2048]{2,1,0:T(8,128)(2,1)} all-to-all(bf16[4,96,2048]{2,1,0:T(8,128)(2,1)S(1)} %bitcast.62), channel_id=1, replica_groups=mesh['ep'=4,'tp'=8] {'ep'}, dimensions={0} | all-to-all | bytes 3145728 | tf_op jit(solution)/shard_map/all_to_all | solution.py:115
  120.7 5.7 %fusion.24 = f32[384,1024]{1,0:T(8,128)} fusion(bf16[384,2048]{1,0:T(8,128)(2,1)} %bitcast.63, bf16[1,2048,1024]{2,1,0:T(8,128)(2,1)} %all-gather.10.cloned.1.call-done), kind=kOutput, calls=%fused_computation.38 | convolution fusion | flops 1610612736 | bytes 7340032 | tf_op jit(solution)/shard_map/jrd,jdf->jrf/dot_general | solution.py:123
  126.4 38.6 %all-gather.12.cloned.1.call-done = bf16[1,2048,1024]{2,1,0:T(8,128)(2,1)} async-done(((bf16[1,2048,128]{2,1,0:T(8,128)(2,1)}), bf16[1,2048,1024]{2,1,0:T(8,128)(2,1)}) %all-gather.12.cloned.1.call-update) | async-done | bytes 4194320 | tf_op jit(solution)/shard_map/all_gather | solution.py:121
  165.0 47.5 %all-gather.14.cloned.1.call-done = bf16[1,2048,1024]{2,1,0:T(8,128)(2,1)} async-done(((bf16[1,2048,128]{2,1,0:T(8,128)(2,1)}), bf16[1,2048,1024]{2,1,0:T(8,128)(2,1)}) %all-gather.14.cloned.1.call-update) | async-done | bytes 4194320 | tf_op jit(solution)/shard_map/all_gather | solution.py:122
  212.5 8.6 %fusion.26 = bf16[384,2048]{1,0:T(8,128)(2,1)} fusion(bf16[1,2048,1024]{2,1,0:T(8,128)(2,1)} %all-gather.14.cloned.1.call-done, f32[384,1024]{1,0:T(8,128)} %fusion.24, bf16[384,2048]{1,0:T(8,128)(2,1)S(1)} %bitcast.64, bf16[1,2048,1024]{2,1,0:T(8,128)(2,1)} %all-gather.12.cloned.1.call-done), kind=kOutput, calls=%fused_computation.41 | convolution fusion | flops 3224371200 | bytes 13107200 | tf_op jit(solution)/shard_map/jrf,jdf->jrd/dot_general | solution.py:128
  221.1 3.8 %all-to-all-start.1 = ((bf16[4,96,2048]{2,1,0:T(8,128)(2,1)}), bf16[4,96,2048]{2,1,0:T(8,128)(2,1)S(1)}, u32[]{:S(2)}, u32[]{:S(2)}) async-start(bf16[4,96,2048]{2,1,0:T(8,128)(2,1)} %bitcast.65), calls=%async_computation.2 | async-start | bytes 3145728 | tf_op jit(solution)/shard_map/all_to_all | solution.py:135
  224.9 0.1 copy.29
  225.0 19.7 %all-to-all-done.1 = bf16[4,96,2048]{2,1,0:T(8,128)(2,1)S(1)} async-done(((bf16[4,96,2048]{2,1,0:T(8,128)(2,1)}), bf16[4,96,2048]{2,1,0:T(8,128)(2,1)S(1)}, u32[]{:S(2)}, u32[]{:S(2)}) %all-to-all-start.1) | async-done | bytes 1572896 | tf_op jit(solution)/shard_map/all_to_all | solution.py:135
  244.7 2.3 gather_fusion.1
  247.1 2.4 reshape.163
  249.4 3.9 %multiply_reduce_fusion = bf16[128,2048]{1,0:T(8,128)(2,1)} fusion(f32[128,2,2048]{2,1,0:T(2,128)S(1)} %reshape.163, f32[128,2]{1,0:T(8,128)S(1)} %copy.29), kind=kLoop, calls=%fused_computation.42 | loop fusion | flops 786432 | bytes 2622464 | tf_op jit(solution)/shard_map/reduce_sum | solution.py:140
  (55 shorter events, 0.4 us)
Async XLA Ops:
  7.2 72.7 %copy-start = (bf16[2,128,2048]{2,1,0:T(8,128)(2,1)S(1)}, bf16[2,128,2048]{2,1,0:T(8,128)(2,1)}, u32[]{:S(2)}) copy-start(bf16[2,128,2048]{2,1,0:T(8,128)(2,1)} %param.23) | copy-start | bytes 3145732
  7.2 5.6 %copy-start.6 = (s32[128,2]{0,1:T(2,128)S(1)}, s32[128,2]{0,1:T(2,128)}, u32[]{:S(2)}) copy-start(s32[128,2]{0,1:T(2,128)} %param.26) | copy-start | bytes 3076
  7.2 6.0 %copy-start.4 = (bf16[512,2,128]{2,1,0:T(2,128)(2,1)S(1)}, bf16[512,2,128]{2,1,0:T(2,128)(2,1)}, u32[]{:S(2)}) copy-start(bf16[512,2,128]{2,1,0:T(2,128)(2,1)} %param.18) | copy-start | bytes 786436
  7.2 9.5 %copy-start.1 = (bf16[128,2048]{1,0:T(8,128)(2,1)S(1)}, bf16[128,2048]{1,0:T(8,128)(2,1)}, u32[]{:S(2)}) copy-start(bf16[128,2048]{1,0:T(8,128)(2,1)} %param.24) | copy-start | bytes 1572868
  7.2 32.5 %all-gather.6.cloned.1.call-start = ((), (), s32[]{:S(2)}) async-start(), calls=%async_computation.3 | async-start | bytes 1310720 | tf_op jit(solution)/shard_map/all_gather | solution.py:53
  9.1 7.9 %copy-start.5 = (f32[2048]{0:T(1024)S(1)}, f32[2048]{0:T(1024)}, u32[]{:S(2)}) copy-start(f32[2048]{0:T(1024)} %param.25) | copy-start | bytes 24580
  9.1 59.0 %all-gather.8.cloned.1.call-start = ((), (), s32[]{:S(2)}) async-start(), calls=%async_computation.4 | async-start | bytes 1310720 | tf_op jit(solution)/shard_map/all_gather | solution.py:54
  10.8 109.8 %all-gather.10.cloned.1.call-start = ((), (), s32[]{:S(2)}) async-start(), calls=%async_computation.6 | async-start | bytes 4718592 | tf_op jit(solution)/shard_map/all_gather | solution.py:120
  11.6 153.4 %all-gather.12.cloned.1.call-start = ((), (), s32[]{:S(2)}) async-start(), calls=%async_computation.7 | async-start | bytes 4718592 | tf_op jit(solution)/shard_map/all_gather | solution.py:121
  12.2 200.3 %all-gather.14.cloned.1.call-start = ((), (), s32[]{:S(2)}) async-start(), calls=%async_computation.8 | async-start | bytes 4718592 | tf_op jit(solution)/shard_map/all_gather | solution.py:122
  12.7 240.6 %reduce-scatter.2.cloned.1.call-start = ((), (), s32[]{:S(2)}) async-start(), calls=%async_computation.5 | async-start | bytes 2359296 | tf_op jit(solution)/shard_map/reduce_scatter | solution.py:81
  69.5 9.9 %copy-start.8 = (f32[2]{0:T(128)S(1)}, f32[2]{0:T(128)}, u32[]{:S(2)}) copy-start(f32[2]{0:T(128)} %param.21) | copy-start | bytes 28
  69.5 10.4 %copy-start.9 = (f32[128]{0:T(128)S(1)}, f32[128]{0:T(128)}, u32[]{:S(2)}) copy-start(f32[128]{0:T(128)} %param.22) | copy-start | bytes 1540
  79.9 2.2 copy-start.2
  120.7 91.8 %copy-start.3 = (bf16[4,96,2048]{2,1,0:T(8,128)(2,1)S(1)}, bf16[4,96,2048]{2,1,0:T(8,128)(2,1)}, u32[]{:S(2)}) copy-start(bf16[4,96,2048]{2,1,0:T(8,128)(2,1)} %all_to_all.10) | copy-start | bytes 4718596
  221.1 3.8 %copy-start.7 = (f32[128,2]{0,1:T(2,128)S(1)}, f32[128,2]{0,1:T(2,128)}, u32[]{:S(2)}) copy-start(f32[128,2]{0,1:T(2,128)} %param.28) | copy-start | bytes 3076
  221.1 3.8 %copy-start.10 = (f32[128]{0:T(128)S(1)}, f32[128]{0:T(128)}, u32[]{:S(2)}) copy-start(f32[128]{0:T(128)} %param.27) | copy-start | bytes 1540
  221.1 23.6 %all-to-all-start.1 = ((bf16[4,96,2048]{2,1,0:T(8,128)(2,1)}), bf16[4,96,2048]{2,1,0:T(8,128)(2,1)S(1)}, u32[]{:S(2)}, u32[]{:S(2)}) async-start(bf16[4,96,2048]{2,1,0:T(8,128)(2,1)} %bitcast.65), calls=%async_computation.2 | async-start | bytes 3145728 | tf_op jit(solution)/shard_map/all_to_all | solution.py:135
Sparse Core Ops, SparseCore 0:
  10.4 29.2 all-gather.5
  41.5 26.4 all-gather.7
  69.7 47.8 all-gather.9
  119.0 45.9 all-gather.11
  166.4 45.9 all-gather.13
  215.2 34.1 reduce-scatter.1
where the time goes:
time: 261 us; the launch traced here: 260 us
  waiting for transfers between devices  155 us (59%)
  blocking collectives  36.1 us (14%)
  local copies, waits for them, and re-layouts  20.4 us (8%)
  matrix products  19.2 us (7%)
  between operations  14.4 us (6%)
  other arithmetic  7.89 us (3%)
  starting transfers between devices  4.02 us (2%)
  loops' own time  2.93 us (1%)
    all_gather x1, waiting for transfers between devices, expert_half(): piece_down = lax.all_gather(down_weight, 'tp', axis=2, tiled=True)  47.5 us
    all_gather x1, waiting for transfers between devices, expert_half(): piece_up = lax.all_gather(up_weight, 'tp', axis=2, tiled=True)  38.6 us
    all_to_all x1, blocking collectives, expert_half(): lax.all_to_all(outgoing, 'ep', split_axis=0, concat_axis=0, tiled=True)  36.1 us
    all_gather x1, waiting for transfers between devices, attend_heads(): value_piece = lax.all_gather(values, 'ep', axis=0, tiled=True)  26.1 us
    all_gather x1, waiting for transfers between devices, attend_heads(): key_piece = lax.all_gather(keys, 'ep', axis=0, tiled=True)  21.8 us
    all_to_all x1, waiting for transfers between devices, expert_half(): lax.all_to_all(outbound, 'ep', split_axis=0, concat_axis=0, tiled=True)  19.7 us
    dot_general x1, matrix products, expert_half(): jnp.einsum('jrf,jdf->jrd', hidden, piece_down, preferred_element_type=jnp...  8.63 us
    unnamed x28, local copies, waits for them, and re-layouts  7.42 us
  transfers between devices with their start and end apart: 7, of which 5 were waited for; matrix products, arithmetic and copies ran while one was open for 18% of the time, Pallas kernels for 0%

commit v1 on v0

--- a/solution.py
+++ b/solution.py
@@ -118,12 +118,25 @@
     )
     expert_rows = expert_rows.reshape(local_count, ep_count * capacity, width)
     piece_gate = lax.all_gather(gate_weight, "tp", axis=2, tiled=True)
-    piece_up = lax.all_gather(up_weight, "tp", axis=2, tiled=True)
     piece_down = lax.all_gather(down_weight, "tp", axis=2, tiled=True)
     gate_part = jnp.einsum(
         "jrd,jdf->jrf", expert_rows, piece_gate, preferred_element_type=jnp.float32
     )
-    up_part = jnp.einsum("jrd,jdf->jrf", expert_rows, piece_up, preferred_element_type=jnp.float32)
+    x = up_weight
+    ways, here, turn = (lax.axis_size("tp"), lax.axis_index("tp"), x.shape[2])
+    results = []
+    for far in range(ways):
+        arriving = (
+            lax.ppermute(x, "tp", [(d, (d + 1) % ways) for d in range(ways)])
+            if far + 1 < ways
+            else x
+        )
+        results.append(
+            jnp.einsum("jrd,jdf->jrf", expert_rows, x, preferred_element_type=jnp.float32)
+        )
+        x = arriving
+    line = jnp.concatenate(results[::-1], axis=2)
+    up_part = jnp.roll(line, (here + 1) * results[0].shape[2], axis=2)
     hidden = (jax.nn.silu(gate_part) * up_part).astype(jnp.bfloat16)
     expert_out = jnp.einsum(
         "jrf,jdf->jrd", hidden, piece_down, preferred_element_type=jnp.float32

time: 261 us -> 231 us (0.89)
  blocking collectives: 36.1 us -> 0 us
  waiting for transfers between devices: 155 us -> 140 us
  local copies, waits for them, and re-layouts: 20.4 us -> 29.8 us
  matrix products: 19.2 us -> 27 us
  starting transfers between devices: 4.02 us -> 9.23 us
    ppermute x0 -> x7, waiting for transfers between devices: none -> 60.9 us  [expert_half(): lax.ppermute(x, 'tp', [(d, (d + 1) % ways) for d in range(ways)])]
    all_gather x1, waiting for transfers between devices: 47.5 us -> 0.01 us  [expert_half(): piece_down = lax.all_gather(down_weight, 'tp', axis=2, tiled=True)]
    all_gather x1, waiting for transfers between devices: 0.01 us -> 45.6 us  [expert_half(): piece_gate = lax.all_gather(gate_weight, 'tp', axis=2, tiled=True)]
    all_gather x1 -> x0, waiting for transfers between devices: 38.6 us -> none  [expert_half(): piece_up = lax.all_gather(up_weight, 'tp', axis=2, tiled=True)]
    all_to_all x1 -> x0, blocking collectives: 36.1 us -> none  [expert_half(): lax.all_to_all(outgoing, 'ep', split_axis=0, concat_axis=0, tiled=True)]
    all_gather x1, waiting for transfers between devices: 21.8 us -> 0.01 us  [attend_heads(): key_piece = lax.all_gather(keys, 'ep', axis=0, tiled=True)]
    all_gather x1, waiting for transfers between devices: 26.1 us -> 12.2 us  [attend_heads(): value_piece = lax.all_gather(values, 'ep', axis=0, tiled=True)]
    dot_general x1 -> x8, matrix products: 5.74 us -> 13.5 us  [expert_half(): jnp.einsum('jrd,jdf->jrf', expert_rows, x, preferred_element_type=jnp.flo...]
  transfers between devices with their start and end apart: 7 -> 14, of which waited for: 5 -> 9; matrix products, arithmetic and copies ran while one was open for 18% -> 27% of each run, Pallas kernels for 0% -> 0%
where the time goes in v1:
time: 231 us
  waiting for transfers between devices  140 us (61%)
  local copies, waits for them, and re-layouts  29.8 us (13%)
  matrix products  27 us (12%)
  between operations  14.1 us (6%)
  starting transfers between devices  9.23 us (4%)
  other arithmetic  8.14 us (4%)
  loops' own time  2.9 us (1%)
    ppermute x7, waiting for transfers between devices, expert_half(): lax.ppermute(x, 'tp', [(d, (d + 1) % ways) for d in range(ways)])  60.9 us
    all_gather x1, waiting for transfers between devices, expert_half(): piece_gate = lax.all_gather(gate_weight, 'tp', axis=2, tiled=True)  45.6 us
    all_to_all x1, waiting for transfers between devices, expert_half(): lax.all_to_all(outbound, 'ep', split_axis=0, concat_axis=0, tiled=True)  19.5 us
    unnamed x49, local copies, waits for them, and re-layouts  14.1 us
    dot_general x8, matrix products, expert_half(): jnp.einsum('jrd,jdf->jrf', expert_rows, x, preferred_element_type=jnp.flo...  13.5 us
    all_gather x1, waiting for transfers between devices, attend_heads(): value_piece = lax.all_gather(values, 'ep', axis=0, tiled=True)  12.2 us
    dot_general x1, matrix products, expert_half(): jnp.einsum('jrf,jdf->jrd', hidden, piece_down, preferred_element_type=jnp...  8.57 us
  transfers between devices with their start and end apart: 14, of which 9 were waited for; matrix products, arithmetic and copies ran while one was open for 27% of the time, Pallas kernels for 0%

profile of v1, /device:TPU:0, one launch (start us, length us, event | category | flops | bytes accessed | tf_op | source)
XLA Modules:
  0.0 230.7 jit_solution(12971844217372385272)
XLA Ops:
  7.3 1.8 copy.32
  9.2 1.7 copy.33
  10.9 0.7 all-gather.11.cloned.1.call-update
  11.7 0.5 all-gather.9.cloned.1.call-update
  12.2 0.5 collective-permute-start
  13.0 10.6 %collective-permute-done = bf16[1,2048,128]{2,1,0:T(8,128)(2,1)S(1)} collective-permute-done((bf16[1,2048,128]{2,1,0:T(8,128)(2,1)S(1)}, bf16[1,2048,128]{2,1,0:T(8,128)(2,1)S(1)}, u32[]{:S(2)}, u32[]{:S(2)}) %collective-permute-start) | collective-permute-done | bytes 524320 | tf_op jit(solution)/shard_map/ppermute | solution.py:130
  23.6 0.2 fusion.33
  23.9 10.2 %collective-permute-done.1 = bf16[1,2048,128]{2,1,0:T(8,128)(2,1)S(1)} collective-permute-done((bf16[1,2048,128]{2,1,0:T(8,128)(2,1)S(1)}, bf16[1,2048,128]{2,1,0:T(8,128)(2,1)S(1)}, u32[]{:S(2)}, u32[]{:S(2)}) %collective-permute-start.1) | collective-permute-done | bytes 524320 | tf_op jit(solution)/shard_map/ppermute | solution.py:130
  34.2 1.2 reduce-window.6
  35.9 0.1 mul.173
  36.0 0.2 fusion.35
  36.3 8.2 %collective-permute-done.2 = bf16[1,2048,128]{2,1,0:T(8,128)(2,1)S(1)} collective-permute-done((bf16[1,2048,128]{2,1,0:T(8,128)(2,1)S(1)}, bf16[1,2048,128]{2,1,0:T(8,128)(2,1)S(1)}, u32[]{:S(2)}, u32[]{:S(2)}) %collective-permute-start.2) | collective-permute-done | bytes 524320 | tf_op jit(solution)/shard_map/ppermute | solution.py:130
  44.6 10.4 %collective-permute-done.3 = bf16[1,2048,128]{2,1,0:T(8,128)(2,1)} collective-permute-done((bf16[1,2048,128]{2,1,0:T(8,128)(2,1)S(1)}, bf16[1,2048,128]{2,1,0:T(8,128)(2,1)}, u32[]{:S(2)}, u32[]{:S(2)}) %collective-permute-start.3) | collective-permute-done | bytes 524320 | tf_op jit(solution)/shard_map/ppermute | solution.py:130
  55.0 1.4 scatter_custom_fusion
  56.4 3.1 %gather_fusion = bf16[384,2048]{1,0:T(8,128)(2,1)} fusion(bf16[129,2048]{1,0:T(8,128)(2,1)S(1)} %concatenate.9, s32[1024]{0:T(1024)S(1)} %pad_clamp_fusion.1), kind=kCustom, calls=%fused_computation | custom fusion | bytes 3147264 | tf_op jit(solution)/shard_map/gather | solution.py:114
  59.5 4.4 %all-to-all-start = ((bf16[4,96,2048]{2,1,0:T(8,128)(2,1)}), bf16[4,96,2048]{2,1,0:T(8,128)(2,1)S(1)}, u32[]{:S(2)}, u32[]{:S(2)}) async-start(bf16[4,96,2048]{2,1,0:T(8,128)(2,1)} %bitcast.145), calls=%async_computation.1 | async-start | bytes 3145728 | tf_op jit(solution)/shard_map/all_to_all | solution.py:115
  63.9 1.8 collective-permute-done.4
  65.7 0.9 copy.35
  66.5 2.3 %copy.34 = bf16[4,512,2,128]{1,3,2,0:T(8,128)(2,1)} copy(bf16[4,512,2,128]{3,1,0,2:T(8,128)(2,1)} %bitcast.147) | data formatting | bytes 2097152
  68.9 12.2 %all-gather.7.cloned.1.call-done = bf16[2048,2,128]{2,0,1:T(8,128)(2,1)} async-done(((bf16[512,2,128]{2,0,1:T(8,128)(2,1)}), bf16[2048,2,128]{2,0,1:T(8,128)(2,1)}) %all-gather.7.cloned.1.call-update) | async-done | bytes 1048592 | tf_op jit(solution)/shard_map/all_gather | solution.py:54
  81.1 2.3 copy.36
  83.4 0.8 broadcast_in_dim.41.clone
  84.3 10.3 %while.23 = (s32[]{:T(128)}, f32[2,512]{1,0:T(2,128)S(1)}, f32[2,512]{1,0:T(2,128)S(1)}, f32[2,512,128]{2,1,0:T(8,128)S(1)}, f32[2,512]{1,0:T(2,128)S(1)}, /*ind...) while((s32[]{:T(128)}, f32[2,512]{1,0:T(2,128)S(1)}, ...), condition=%wide.region_7.8_spmd.clone, body=%wide.region_0.7_spmd.clone.sunk | while | flops 410784768 | bytes 25571820 | solution.py:70
  84.3 0.6 dynamic_slice.46
  85.6 5.2 %conditional.3 = ((f32[2,512]{1,0:T(2,128)S(1)}, f32[2,512]{1,0:T(2,128)S(1)}, f32[2,512,128]{2,1,0:T(8,128)S(1)}, f32[2,512]{1,0:T(2,128)S(1)}, f32[2,512]{1,0:T(2,128)S(1)}, /*index=5*/f32[2,512,128]{2,1,0:T(8,128)})) conditional(s32[]{:T(128)} %convert_element_type.88, (f32[2,512]{1,0:T(2,128)S(1)}, f32[2,512]{1,0:T(2,128)S(1)}, ...), branch_computations={%region_1.1_spmd, %region_2.6_spmd} | conditional | flops 410784768 | bytes 25569440 | solution.py:62
  85.6 1.0 dynamic-slice_bitcast_fusion
  86.6 0.2 broadcast_compare_fusion
  86.8 0.6 fusion.56
  87.4 0.3 fusion.3
  87.8 0.6 fusion.57
  88.4 0.3 fusion.5
  88.8 0.4 copy-done.3
  89.2 0.7 convolution_add_fusion
  89.9 0.7 convolution_add_fusion.1
  90.7 0.6 dynamic_slice.46
  92.0 0.6 dynamic_slice.46
  93.3 0.6 dynamic_slice.46
  94.6 1.6 multiply_reduce_fusion.1
  96.2 0.2 collective-permute-start.6
  96.5 2.2 bitcast_convert_fusion
  98.7 19.7 %collective-permute-done.6 = bf16[1,2048,128]{2,1,0:T(8,128)(2,1)S(1)} collective-permute-done((bf16[1,2048,128]{2,1,0:T(8,128)(2,1)}, bf16[1,2048,128]{2,1,0:T(8,128)(2,1)S(1)}, u32[]{:S(2)}, u32[]{:S(2)}) %collective-permute-start.6) | collective-permute-done | bytes 524320 | tf_op jit(solution)/shard_map/ppermute | solution.py:130
  118.4 1.3 constant_dynamic-update-slice_fusion.15
  119.7 2.3 %constant_dynamic-update-slice_fusion.14 = (f32[1,384,2048]{2,1,0:T(8,128)}, f32[1,384,128]{2,1,0:T(8,128)S(1)}) fusion(f32[1,384,2048]{2,1,0:T(8,128)} %get-tuple-element.381, bf16[384,2048]{1,0:T(8,128)(2,1)S(1)} %bitcast.136, bf16[1,2048,128]{2,1,0:T(8,128)(2,1)} %collective-permute-done.5), kind=kOutput, calls=%fused_computation.85 | convolution fusion | flops 201326592 | bytes 2490368 | tf_op jit(solution)/shard_map/jrd,jdf->jrf/dot_general | solution.py:135
  122.0 2.4 %constant_dynamic-update-slice_fusion.13 = (f32[1,384,2048]{2,1,0:T(8,128)}, f32[1,384,128]{2,1,0:T(8,128)S(1)}) fusion(f32[1,384,2048]{2,1,0:T(8,128)} %get-tuple-element.383, bf16[384,2048]{1,0:T(8,128)(2,1)S(1)} %bitcast.137, bf16[1,2048,128]{2,1,0:T(8,128)(2,1)} %collective-permute-done.4), kind=kOutput, calls=%fused_computation.84 | convolution fusion | flops 201326592 | bytes 2490368 | tf_op jit(solution)/shard_map/jrd,jdf->jrf/dot_general | solution.py:135
  124.4 2.4 %constant_dynamic-update-slice_fusion.12 = (f32[1,384,2048]{2,1,0:T(8,128)}, f32[1,384,128]{2,1,0:T(8,128)S(1)}) fusion(f32[1,384,2048]{2,1,0:T(8,128)} %get-tuple-element.385, bf16[384,2048]{1,0:T(8,128)(2,1)S(1)} %bitcast.138, bf16[1,2048,128]{2,1,0:T(8,128)(2,1)} %collective-permute-done.3), kind=kOutput, calls=%fused_computation.83 | convolution fusion | flops 201326592 | bytes 2490368 | tf_op jit(solution)/shard_map/jrd,jdf->jrf/dot_general | solution.py:135
  126.8 1.3 constant_dynamic-update-slice_fusion.11
  128.0 1.3 constant_dynamic-update-slice_fusion.10
  129.3 1.3 constant_dynamic-update-slice_fusion.9
  130.6 1.3 constant_dynamic-update-slice_fusion.8
  131.9 0.7 constant_dynamic-update-slice_fusion.7
  132.6 0.7 constant_dynamic-update-slice_fusion.6
  133.3 0.7 constant_dynamic-update-slice_fusion.5
  134.1 0.7 constant_dynamic-update-slice_fusion.4
  134.8 0.7 constant_dynamic-update-slice_fusion.3
  135.5 0.7 constant_dynamic-update-slice_fusion.2
  136.2 0.7 constant_dynamic-update-slice_fusion.1
  136.9 0.7 constant_dynamic-update-slice_fusion
  137.6 45.6 %all-gather.9.cloned.1.call-done = bf16[1,2048,1024]{2,1,0:T(8,128)(2,1)} async-done(((bf16[1,2048,128]{2,1,0:T(8,128)(2,1)}), bf16[1,2048,1024]{2,1,0:T(8,128)(2,1)}) %all-gather.9.cloned.1.call-update) | async-done | bytes 4194320 | tf_op jit(solution)/shard_map/all_gather | solution.py:120
  183.3 8.6 %fusion.24 = bf16[384,2048]{1,0:T(8,128)(2,1)} fusion(bf16[1,2048,1024]{2,1,0:T(8,128)(2,1)} %all-gather.11.cloned.1.call-done, f32[1,384,2048]{2,1,0:T(8,128)} %constant_dynamic-update-slice_fusion, s32[]{:T(128)S(6)} %select_n.47, bf16[384,2048]{1,0:T(8,128)(2,1)S(1)} %bitcast.143, bf16[1,2048,1024]{2,1,0:T(8,128)(2,1)} %all-gather.9.cloned.1.call-done), kind=kOutput, calls=%fused_computation.39 | convolution fusion | flops 3224371200 | bytes 13107204 | tf_op jit(solution)/shard_map/jrf,jdf->jrd/dot_general | solution.py:141
  191.8 3.9 %all-to-all-start.1 = ((bf16[4,96,2048]{2,1,0:T(8,128)(2,1)}), bf16[4,96,2048]{2,1,0:T(8,128)(2,1)S(1)}, u32[]{:S(2)}, u32[]{:S(2)}) async-start(bf16[4,96,2048]{2,1,0:T(8,128)(2,1)} %bitcast.146), calls=%async_computation.2 | async-start | bytes 3145728 | tf_op jit(solution)/shard_map/all_to_all | solution.py:148
  195.9 19.5 %all-to-all-done.1 = bf16[4,96,2048]{2,1,0:T(8,128)(2,1)S(1)} async-done(((bf16[4,96,2048]{2,1,0:T(8,128)(2,1)}), bf16[4,96,2048]{2,1,0:T(8,128)(2,1)S(1)}, u32[]{:S(2)}, u32[]{:S(2)}) %all-to-all-start.1) | async-done | bytes 1572896 | tf_op jit(solution)/shard_map/all_to_all | solution.py:148
  215.5 2.4 %gather_fusion.1 = bf16[256,2048]{1,0:T(8,128)(2,1)} fusion(bf16[384,2048]{1,0:T(8,128)(2,1)S(1)} %bitcast.144, s32[1024]{0:T(1024)S(1)} %pad_clamp_fusion), kind=kCustom, calls=%fused_computation.1 | custom fusion | bytes 2098176 | tf_op jit(solution)/shard_map/gather | solution.py:151
  217.8 2.4 %reshape.212 = f32[128,2,2048]{2,1,0:T(2,128)S(1)} reshape(bf16[256,2048]{1,0:T(8,128)(2,1)} %gather_fusion.1) | data formatting | bytes 3145728 | tf_op jit(solution)/shard_map/convert_element_type | solution.py:151
  220.2 3.9 %multiply_reduce_fusion = bf16[128,2048]{1,0:T(8,128)(2,1)} fusion(f32[128,2,2048]{2,1,0:T(2,128)S(1)} %reshape.212, f32[128,2]{1,0:T(8,128)S(1)} %copy.37), kind=kLoop, calls=%fused_computation.40 | loop fusion | flops 786432 | bytes 2622464 | tf_op jit(solution)/shard_map/reduce_sum | solution.py:153
  (102 shorter events, 1.7 us)
Async XLA Ops:
  7.2 89.3 %copy-start = (bf16[2,128,2048]{2,1,0:T(8,128)(2,1)S(1)}, bf16[2,128,2048]{2,1,0:T(8,128)(2,1)}, u32[]{:S(2)}) copy-start(bf16[2,128,2048]{2,1,0:T(8,128)(2,1)} %param.23) | copy-start | bytes 3145732
  7.2 5.0 %copy-start.5 = (bf16[1,2048,128]{2,1,0:T(8,128)(2,1)S(1)}, bf16[1,2048,128]{2,1,0:T(8,128)(2,1)}, u32[]{:S(2)}) copy-start(bf16[1,2048,128]{2,1,0:T(8,128)(2,1)} %param.30) | copy-start | bytes 1572868
  7.2 5.6 %copy-start.16 = (s32[128,2]{0,1:T(2,128)S(1)}, s32[128,2]{0,1:T(2,128)}, u32[]{:S(2)}) copy-start(s32[128,2]{0,1:T(2,128)} %param.26) | copy-start | bytes 3076
  7.2 16.4 %copy-start.4 = (bf16[128,2048]{1,0:T(8,128)(2,1)S(1)}, bf16[128,2048]{1,0:T(8,128)(2,1)}, u32[]{:S(2)}) copy-start(bf16[128,2048]{1,0:T(8,128)(2,1)} %param.24) | copy-start | bytes 1572868
  7.2 28.8 %copy-start.15 = (f32[2048]{0:T(1024)S(1)}, f32[2048]{0:T(1024)}, u32[]{:S(2)}) copy-start(f32[2048]{0:T(1024)} %param.25) | copy-start | bytes 24580
  7.2 59.3 %all-gather.5.cloned.1.call-start = ((), (), s32[]{:S(2)}) async-start(), calls=%async_computation.3 | async-start | bytes 1310720 | tf_op jit(solution)/shard_map/all_gather | solution.py:53
  9.1 72.0 %all-gather.7.cloned.1.call-start = ((), (), s32[]{:S(2)}) async-start(), calls=%async_computation.4 | async-start | bytes 1310720 | tf_op jit(solution)/shard_map/all_gather | solution.py:54
  10.9 126.8 %all-gather.11.cloned.1.call-start = ((), (), s32[]{:S(2)}) async-start(), calls=%async_computation.7 | async-start | bytes 4718592 | tf_op jit(solution)/shard_map/all_gather | solution.py:121
  11.6 171.7 %all-gather.9.cloned.1.call-start = ((), (), s32[]{:S(2)}) async-start(), calls=%async_computation.6 | async-start | bytes 4718592 | tf_op jit(solution)/shard_map/all_gather | solution.py:120
  12.2 11.4 %collective-permute-start = (bf16[1,2048,128]{2,1,0:T(8,128)(2,1)S(1)}, bf16[1,2048,128]{2,1,0:T(8,128)(2,1)S(1)}, u32[]{:S(2)}, u32[]{:S(2)}) collective-permute-start(bf16[1,2048,128]{2,1,0:T(8,128)(2,1)S(1)} %copy-done.5), channel_id=1, source_target_pairs={{0,1},{1,2},{2,3},{3,4},{4,5},{5,6},{6,7},{7,0},{8,9},{9,10},{10,1... | collective-permute-start | bytes 1572872 | tf_op jit(solution)/shard_map/ppermute | solution.py:130
  23.6 35.9 %copy-start.7 = (bf16[1,2048,128]{2,1,0:T(8,128)(2,1)}, bf16[1,2048,128]{2,1,0:T(8,128)(2,1)S(1)}, u32[]{:S(2)}) copy-start(bf16[1,2048,128]{2,1,0:T(8,128)(2,1)S(1)} %collective-permute-done) | copy-start | bytes 1572868
  23.6 10.4 %collective-permute-start.1 = (bf16[1,2048,128]{2,1,0:T(8,128)(2,1)S(1)}, bf16[1,2048,128]{2,1,0:T(8,128)(2,1)S(1)}, u32[]{:S(2)}, u32[]{:S(2)}) collective-permute-start(bf16[1,2048,128]{2,1,0:T(8,128)(2,1)S(1)} %collective-permute-done), channel_id=1, source_target_pairs={{0,1},{1,2},{2,3},{3,4},{4,5},{5,6},{6,7},{7,0},{8,9},{9,10},{10,1... | collective-permute-start | bytes 1572872 | tf_op jit(solution)/shard_map/ppermute | solution.py:130
  34.0 25.5 %copy-start.9 = (bf16[1,2048,128]{2,1,0:T(8,128)(2,1)}, bf16[1,2048,128]{2,1,0:T(8,128)(2,1)S(1)}, u32[]{:S(2)}) copy-start(bf16[1,2048,128]{2,1,0:T(8,128)(2,1)S(1)} %collective-permute-done.1) | copy-start | bytes 1572868
  34.0 10.4 %collective-permute-start.2 = (bf16[1,2048,128]{2,1,0:T(8,128)(2,1)S(1)}, bf16[1,2048,128]{2,1,0:T(8,128)(2,1)S(1)}, u32[]{:S(2)}, u32[]{:S(2)}) collective-permute-start(bf16[1,2048,128]{2,1,0:T(8,128)(2,1)S(1)} %collective-permute-done.1), channel_id=1, source_target_pairs={{0,1},{1,2},{2,3},{3,4},{4,5},{5,6},{6,7},{7,0},{8,9},{9,10},{10,1... | collective-permute-start | bytes 1572872 | tf_op jit(solution)/shard_map/ppermute | solution.py:130
  44.5 15.1 %copy-start.11 = (bf16[1,2048,128]{2,1,0:T(8,128)(2,1)}, bf16[1,2048,128]{2,1,0:T(8,128)(2,1)S(1)}, u32[]{:S(2)}) copy-start(bf16[1,2048,128]{2,1,0:T(8,128)(2,1)S(1)} %collective-permute-done.2) | copy-start | bytes 1572868
  44.5 10.5 %collective-permute-start.3 = (bf16[1,2048,128]{2,1,0:T(8,128)(2,1)S(1)}, bf16[1,2048,128]{2,1,0:T(8,128)(2,1)}, u32[]{:S(2)}, u32[]{:S(2)}) collective-permute-start(bf16[1,2048,128]{2,1,0:T(8,128)(2,1)S(1)} %collective-permute-done.2), channel_id=1, source_target_pairs={{0,1},{1,2},{2,3},{3,4},{4,5},{5,6},{6,7},{7,0},{8,9},{9,10},{10,1... | collective-permute-start | bytes 1572872 | tf_op jit(solution)/shard_map/ppermute | solution.py:130
  55.0 10.7 %collective-permute-start.4 = (bf16[1,2048,128]{2,1,0:T(8,128)(2,1)}, bf16[1,2048,128]{2,1,0:T(8,128)(2,1)}, u32[]{:S(2)}, u32[]{:S(2)}) collective-permute-start(bf16[1,2048,128]{2,1,0:T(8,128)(2,1)} %collective-permute-done.3), channel_id=1, source_target_pairs={{0,1},{1,2},{2,3},{3,4},{4,5},{5,6},{6,7},{7,0},{8,9},{9,10},{10,1... | collective-permute-start | bytes 1572872 | tf_op jit(solution)/shard_map/ppermute | solution.py:130
  59.5 6.2 %copy-start.13 = (bf16[512,2,128]{2,1,0:T(2,128)(2,1)S(1)}, bf16[512,2,128]{2,1,0:T(2,128)(2,1)}, u32[]{:S(2)}) copy-start(bf16[512,2,128]{2,1,0:T(2,128)(2,1)} %param.18) | copy-start | bytes 786436
  59.5 39.2 %all-to-all-start = ((bf16[4,96,2048]{2,1,0:T(8,128)(2,1)}), bf16[4,96,2048]{2,1,0:T(8,128)(2,1)S(1)}, u32[]{:S(2)}, u32[]{:S(2)}) async-start(bf16[4,96,2048]{2,1,0:T(8,128)(2,1)} %bitcast.145), calls=%async_computation.1 | async-start | bytes 3145728 | tf_op jit(solution)/shard_map/all_to_all | solution.py:115
  63.9 160.3 %reduce-scatter.2.cloned.1.call-start = ((), (), s32[]{:S(2)}) async-start(), calls=%async_computation.5 | async-start | bytes 2359296 | tf_op jit(solution)/shard_map/reduce_scatter | solution.py:81
  65.7 30.5 %collective-permute-start.5 = (bf16[1,2048,128]{2,1,0:T(8,128)(2,1)}, bf16[1,2048,128]{2,1,0:T(8,128)(2,1)}, u32[]{:S(2)}, u32[]{:S(2)}) collective-permute-start(bf16[1,2048,128]{2,1,0:T(8,128)(2,1)} %collective-permute-done.4), channel_id=1, source_target_pairs={{0,1},{1,2},{2,3},{3,4},{4,5},{5,6},{6,7},{7,0},{8,9},{9,10},{10,1... | collective-permute-start | bytes 1572872 | tf_op jit(solution)/shard_map/ppermute | solution.py:130
  68.9 15.4 %copy-start.14 = (bf16[512,2,128]{0,2,1:T(8,128)(2,1)S(1)}, bf16[512,2,128]{0,2,1:T(8,128)(2,1)}, u32[]{:S(2)}) copy-start(bf16[512,2,128]{0,2,1:T(8,128)(2,1)} %copy.35) | copy-start | bytes 786436
  84.3 10.4 %copy-start.18 = (f32[2]{0:T(128)S(1)}, f32[2]{0:T(128)}, u32[]{:S(2)}) copy-start(f32[2]{0:T(128)} %param.21) | copy-start | bytes 28
  84.3 12.2 %copy-start.19 = (f32[128]{0:T(128)S(1)}, f32[128]{0:T(128)}, u32[]{:S(2)}) copy-start(f32[128]{0:T(128)} %param.22) | copy-start | bytes 1540
  87.7 1.1 copy-start.1
  87.8 1.5 copy-start.3
  89.9 0.8 copy-start.2
  96.2 22.2 %collective-permute-start.6 = (bf16[1,2048,128]{2,1,0:T(8,128)(2,1)}, bf16[1,2048,128]{2,1,0:T(8,128)(2,1)S(1)}, u32[]{:S(2)}, u32[]{:S(2)}) collective-permute-start(bf16[1,2048,128]{2,1,0:T(8,128)(2,1)} %collective-permute-done.5), channel_id=1, source_target_pairs={{0,1},{1,2},{2,3},{3,4},{4,5},{5,6},{6,7},{7,0},{8,9},{9,10},{10,1... | collective-permute-start | bytes 1572872 | tf_op jit(solution)/shard_map/ppermute | solution.py:130
  122.0 4.8 %copy-start.12 = (bf16[1,2048,128]{2,1,0:T(8,128)(2,1)S(1)}, bf16[1,2048,128]{2,1,0:T(8,128)(2,1)}, u32[]{:S(2)}) copy-start(bf16[1,2048,128]{2,1,0:T(8,128)(2,1)} %copy-done.11) | copy-start | bytes 1572868
  124.4 3.7 %copy-start.10 = (bf16[1,2048,128]{2,1,0:T(8,128)(2,1)S(1)}, bf16[1,2048,128]{2,1,0:T(8,128)(2,1)}, u32[]{:S(2)}) copy-start(bf16[1,2048,128]{2,1,0:T(8,128)(2,1)} %copy-done.9) | copy-start | bytes 1572868
  126.8 2.6 %copy-start.8 = (bf16[1,2048,128]{2,1,0:T(8,128)(2,1)S(1)}, bf16[1,2048,128]{2,1,0:T(8,128)(2,1)}, u32[]{:S(2)}) copy-start(bf16[1,2048,128]{2,1,0:T(8,128)(2,1)} %copy-done.7) | copy-start | bytes 1572868
  128.0 2.6 %copy-start.6 = (bf16[1,2048,128]{2,1,0:T(8,128)(2,1)S(1)}, bf16[1,2048,128]{2,1,0:T(8,128)(2,1)}, u32[]{:S(2)}) copy-start(bf16[1,2048,128]{2,1,0:T(8,128)(2,1)} %param.30) | copy-start | bytes 1572868
  191.8 3.9 %copy-start.17 = (f32[128,2]{0,1:T(2,128)S(1)}, f32[128,2]{0,1:T(2,128)}, u32[]{:S(2)}) copy-start(f32[128,2]{0,1:T(2,128)} %param.28) | copy-start | bytes 3076
  191.8 3.9 %copy-start.20 = (f32[128]{0:T(128)S(1)}, f32[128]{0:T(128)}, u32[]{:S(2)}) copy-start(f32[128]{0:T(128)} %param.27) | copy-start | bytes 1540
  191.8 23.6 %all-to-all-start.1 = ((bf16[4,96,2048]{2,1,0:T(8,128)(2,1)}), bf16[4,96,2048]{2,1,0:T(8,128)(2,1)S(1)}, u32[]{:S(2)}, u32[]{:S(2)}) async-start(bf16[4,96,2048]{2,1,0:T(8,128)(2,1)} %bitcast.146), calls=%async_computation.2 | async-start | bytes 3145728 | tf_op jit(solution)/shard_map/all_to_all | solution.py:148
Sparse Core Ops, SparseCore 0:
  10.5 29.2 all-gather.4
  42.1 38.9 all-gather.6
  82.7 53.0 all-gather.10
  137.2 45.9 all-gather.8
  186.0 34.0 reduce-scatter.1
